TPU v7x, 32 devices: a whole 2x2x4 slice. The times are simulated.
32 devices in a mesh: sp: 8 (over z, y), tp: 4 (over x, core).
Axes of the slice: x: 2, y: 2, z: 4, core: 2. Of those that a mesh axis runs over, the one named last changes fastest.
Arguments:
- queries: bfloat16 [5120, 1024], P('sp', 'tp'), may hold values from -6 to 6
- key_input: bfloat16 [5120, 1024], P('sp', 'tp'), may hold values from -6 to 6
- value_input: bfloat16 [5120, 1024], P('sp', 'tp'), may hold values from -6 to 6
- gate_input: bfloat16 [5120, 1024], P('sp', 'tp'), may hold values from -6 to 6
- log_decay: float32 [8, 5120], P('tp', 'sp'), may hold values from -1.6703125 to 0, as said below
- residual: bfloat16 [5120, 2048], P('sp'), may hold values from -52 to 52
- out_weight: bfloat16 [1024, 2048], P('tp'), may hold values from -0.375 to 0.375
- norm_gain: float32 [2048], replicated, may hold values from 0.3 to 2.7, as said below
- norm_bias: float32 [2048], replicated, may hold values from -1.8 to 1.8
- gate_weight: bfloat16 [2048, 5632], P('sp', 'tp'), may hold values from -0.125 to 0.125
- up_weight: bfloat16 [2048, 5632], P('sp', 'tp'), may hold values from -0.125 to 0.125
- down_weight: bfloat16 [5632, 2048], P('tp', 'sp'), may hold values from -0.078125 to 0.078125
- final_gain: float32 [2048], replicated, may hold values from 0.1 to 1.9
- final_bias: float32 [2048], replicated, may hold values from -1.8 to 1.8
Outputs:
- updated: bfloat16 [5120, 2048], P('sp', 'tp')
Inputs may be any that keep to these rules, and one draw needn't show every extreme that they name: `log_decay`: log-decays, never positive. `norm_gain`: positive gains.
All inputs are finite; a program needn't handle non-finite values.
Results may differ from a plain program's by a relative error of at most 0.023.
Values may be sent and summed in bfloat16 or wider, within the bound.
A program may use at most 128 MiB of HBM per device.

v0:
```python
import jax
import jax.numpy as jnp
from jax import lax
from jax.sharding import PartitionSpec as P

HD = 128
BLOCK = 128


ALPHA = 2.0**0.25
EPS = 1e-05
ROPE_BASE = 10000.0


def prefix(x, axis, combine, identity):
    peers, position = (lax.axis_size(axis), lax.axis_index(axis))
    everything = jax.tree.map(
        lambda part, kind: lax.all_gather(part.astype(kind), axis), x, (jnp.bfloat16, jnp.bfloat16)
    )
    start = jax.tree.map(
        lambda part, zero: jnp.broadcast_to(jnp.asarray(zero, part.dtype), part.shape), x, identity
    )

    def hop(k, before):
        reached = k < position
        new = combine(
            before, jax.tree.map(lambda part, own: part[k].astype(own.dtype), everything, x)
        )
        return jax.tree.map(lambda a, b: jnp.where(reached, a, b), new, before)

    return lax.fori_loop(0, peers, hop, start)


def rotate(values, positions):
    half = values.shape[-1] // 2
    freqs = ROPE_BASE ** (-2.0 * jnp.arange(half, dtype=jnp.float32) / values.shape[-1])
    angles = positions[:, None] * freqs[None, :]
    cosine = jnp.cos(angles)[:, None, :]
    sine = jnp.sin(angles)[:, None, :]
    first = values[..., :half]
    latter_operand = values[..., half:]
    return jnp.concatenate(
        [first * cosine - latter_operand * sine, first * sine + latter_operand * cosine], axis=-1
    )


def head_norm(retained):
    center = retained - jnp.mean(retained, axis=-1, keepdims=True)
    spread = jnp.mean(center * center, axis=-1, keepdims=True)
    return center * lax.rsqrt(spread + EPS)


def combine_states(earlier, later):
    return (earlier[0] * later[0], later[1] + later[0][:, None, None] * earlier[1])


def shards(
    queries,
    key_input,
    value_input,
    gate_input,
    log_decay,
    residual,
    out_weight,
    norm_gain,
    norm_bias,
    gate_weight,
    up_weight,
    down_weight,
    final_gain,
    final_bias,
):
    rows = queries.shape[0]
    heads_here = queries.shape[1] // HD
    blocks = rows // BLOCK
    offset = lax.axis_index("sp") * rows
    positions = (offset + jnp.arange(rows, dtype=jnp.int32)).astype(jnp.float32)
    shaped = (rows, heads_here, HD)
    per_block = (blocks, BLOCK, heads_here, HD)
    turned_q = (
        rotate(queries.astype(jnp.float32).reshape(shaped), positions)
        .astype(jnp.bfloat16)
        .reshape(per_block)
    )
    turned_k = (
        rotate(key_input.astype(jnp.float32).reshape(shaped), positions)
        .astype(jnp.bfloat16)
        .reshape(per_block)
    )
    value_blocks = value_input.reshape(per_block)
    cumul = jnp.cumsum(
        jnp.transpose(log_decay.reshape(heads_here, blocks, BLOCK), (1, 0, 2)), axis=2
    )
    cumul_rows = jnp.transpose(cumul, (0, 2, 1))
    lower = jnp.arange(BLOCK)[:, None] >= jnp.arange(BLOCK)[None, :]
    gaps = cumul[:, :, :, None] - cumul[:, :, None, :]
    damping = jnp.where(lower[None, None], jnp.exp(jnp.minimum(gaps, 0.0)), 0.0)
    scores = jnp.einsum("nihd,njhd->nhij", turned_q, turned_k, preferred_element_type=jnp.float32)
    weights = (scores * damping).astype(jnp.bfloat16)
    inner = jnp.einsum("nhij,njhe->nihe", weights, value_blocks, preferred_element_type=jnp.float32)
    ending = cumul[:, :, -1]
    value_broadened = value_blocks.astype(jnp.float32)
    keyed = turned_k.astype(jnp.float32) * jnp.exp(ending[:, None, :] - cumul_rows)[:, :, :, None]
    fresh = jnp.einsum("njhd,njhe->nhde", keyed, value_broadened, precision=lax.Precision.HIGHEST)

    def advance(state, pieces):
        decay_here, fresh_here = pieces
        return (jnp.exp(decay_here)[:, None, None] * state + fresh_here, state)

    local_state, prefixes = lax.scan(
        advance, jnp.zeros((heads_here, HD, HD), jnp.float32), (ending, fresh)
    )
    before = jnp.cumsum(ending, axis=0) - ending
    device_decay = jnp.exp(jnp.sum(ending, axis=0))
    scanned = prefix(
        (device_decay, local_state),
        "sp",
        combine_states,
        (jnp.ones_like(device_decay), jnp.zeros_like(local_state)),
    )
    entering = prefixes + jnp.exp(before)[:, :, None, None] * scanned[1][None]
    query_wide = turned_q.astype(jnp.float32) * jnp.exp(cumul_rows)[:, :, :, None]
    outer = jnp.einsum("nihd,nhde->nihe", query_wide, entering, precision=lax.Precision.HIGHEST)
    normed = head_norm((inner + outer).reshape(shaped)).reshape(rows, heads_here * HD)
    mixed_heads = (jax.nn.silu(gate_input.astype(jnp.float32)) * normed).astype(jnp.bfloat16)
    partial_value = jnp.dot(mixed_heads, out_weight, preferred_element_type=jnp.float32)
    width = residual.shape[1]
    col_width = width // lax.axis_size("tp")
    col_start = lax.axis_index("tp") * col_width

    def own_columns(array):
        return lax.dynamic_slice_in_dim(array, col_start, col_width, array.ndim - 1)

    mix = lax.psum(partial_value.astype(jnp.bfloat16), "tp")
    leading_sum = ALPHA * residual.astype(jnp.float32) + mix.astype(jnp.float32)
    center = leading_sum - jnp.mean(leading_sum, axis=1, keepdims=True)
    spread = jnp.mean(center * center, axis=1, keepdims=True)
    settled = (center * lax.rsqrt(spread + EPS) * norm_gain + norm_bias).astype(jnp.bfloat16)
    settled_cols = own_columns(settled)

    def add_rows(piece):
        return jnp.dot(settled, piece, preferred_element_type=jnp.float32)

    gate_acts = add_rows(lax.all_gather(gate_weight, "sp", axis=0, tiled=True))
    lifted = add_rows(lax.all_gather(up_weight, "sp", axis=0, tiled=True))
    latent_width = (jax.nn.silu(gate_acts) * lifted).astype(jnp.bfloat16)
    terms = jnp.dot(
        latent_width,
        lax.all_gather(down_weight, "sp", axis=1, tiled=True),
        preferred_element_type=jnp.float32,
    )
    ffn_cols = lax.psum_scatter(terms.astype(jnp.bfloat16), "tp", scatter_dimension=1, tiled=True)
    second_sum = ALPHA * settled_cols.astype(jnp.float32) + ffn_cols.astype(jnp.float32)
    totals_two, squares_two = lax.psum(
        (jnp.sum(second_sum, axis=1), jnp.sum(second_sum * second_sum, axis=1)), "tp"
    )
    average_two = totals_two / width
    spread_two = squares_two / width - average_two * average_two
    scaled_two = (second_sum - average_two[:, None]) * lax.rsqrt(spread_two + EPS)[:, None]
    return (scaled_two * own_columns(final_gain) + own_columns(final_bias)).astype(jnp.bfloat16)


def solution(mesh):
    in_specs = (
        P("sp", "tp"),
        P("sp", "tp"),
        P("sp", "tp"),
        P("sp", "tp"),
        P("tp", "sp"),
        P("sp", None),
        P("tp", None),
        P(),
        P(),
        P("sp", "tp"),
        P("sp", "tp"),
        P("tp", "sp"),
        P(),
        P(),
    )
    out_specs = P("sp", "tp")
    return jax.shard_map(shards, mesh=mesh, in_specs=in_specs, out_specs=out_specs, check_vma=False)
```

profile of v0, /device:TPU:16, one launch (start us, length us, event | category | flops | bytes accessed | tf_op | source)
XLA Modules:
  0.0 433.2 jit_solution(10507391402819925788)
XLA Ops:
  7.5 1.2 copy.65
  8.7 1.1 copy.66
  10.5 0.9 subtract_convert_fusion.1
  12.4 1.5 reduce_window_sum.22
  14.5 1.0 fusion.16
  15.5 3.9 while.29
  19.4 26.9 %all-gather = bf16[16,128,128]{2,1,0:T(8,128)(2,1)S(1)} all-gather(bf16[2,128,128]{2,1,0:T(8,128)(2,1)S(1)} %convert_element_type.101), channel_id=2, replica_groups=mesh['sp'=8,'tp'=4] {'sp'}, dimensions={0}, use_global_device_ids=true | all-gather | bytes 589824 | tf_op jit(solution)/shard_map/all_gather | solution.py:18
  48.0 20.6 %all-reduce = bf16[16]{0:T(256)(128)(2,1)S(1)} all-reduce(bf16[16]{0:T(256)(128)(2,1)S(1)} %dynamic-update-slice), channel_id=3, replica_groups=mesh['sp'=8,'tp'=4] {'sp'}, use_global_device_ids=true, to_apply=%add | all-reduce | flops 16 | bytes 64
  68.7 1.0 while.30
  69.7 1.1 concatenate.18
  71.1 1.1 concatenate.19
  72.6 3.5 convolution_bitcast_fusion
  76.0 1.9 fusion.44
  78.0 0.9 copy.60
  79.4 0.8 mul.258
  80.2 0.8 sub.78
  81.0 2.5 convolution_convert_fusion.1
  85.5 60.8 %all-reduce.4.cloned.1.call-done = bf16[640,2048]{1,0:T(8,128)(2,1)} async-done(((bf16[640,2048]{1,0:T(8,128)(2,1)}), bf16[640,2048]{1,0:T(8,128)(2,1)}) %all-reduce.4.cloned.1.call-update) | async-done | bytes 2621456 | tf_op jit(solution)/shard_map/psum | solution.py:134
  146.3 3.6 fusion.3
  150.5 1.3 multiply_reduce_fusion
  151.8 3.0 add_convert_fusion
  154.8 25.4 %all-gather.6.cloned.1.call-done = bf16[2048,1408]{1,0:T(8,128)(2,1)} async-done(((bf16[256,1408]{1,0:T(8,128)(2,1)}), bf16[2048,1408]{1,0:T(8,128)(2,1)}) %all-gather.6.cloned.1.call-update) | async-done | bytes 5767184 | tf_op jit(solution)/shard_map/all_gather | solution.py:144
  180.2 9.4 %fusion.45 = f32[640,1408]{1,0:T(8,128)} fusion(bf16[640,2048]{1,0:T(8,128)(2,1)} %add_convert_fusion, bf16[2048,1408]{1,0:T(8,128)(2,1)} %all-gather.6.cloned.1.call-done), kind=kOutput, calls=%fused_computation.87 | convolution fusion | flops 3690987520 | bytes 11993088 | tf_op jit(solution)/shard_map/dot_general | solution.py:142
  189.6 83.6 %all-gather.10.cloned.1.call-done = bf16[1408,2048]{1,0:T(8,128)(2,1)} async-done(((bf16[1408,256]{1,0:T(8,128)(2,1)}), bf16[1408,2048]{1,0:T(8,128)(2,1)}) %all-gather.10.cloned.1.call-update) | async-done | bytes 5767184 | tf_op jit(solution)/shard_map/all_gather | solution.py:149
  273.2 92.4 %all-gather.8.cloned.1.call-done = bf16[2048,1408]{1,0:T(8,128)(2,1)} async-done(((bf16[256,1408]{1,0:T(8,128)(2,1)}), bf16[2048,1408]{1,0:T(8,128)(2,1)}) %all-gather.8.cloned.1.call-update) | async-done | bytes 5767184 | tf_op jit(solution)/shard_map/all_gather | solution.py:145
  365.6 16.2 %convolution_convert_fusion = bf16[640,2048]{1,0:T(8,128)(2,1)} fusion(bf16[1408,2048]{1,0:T(8,128)(2,1)} %all-gather.10.cloned.1.call-done, bf16[640,2048]{1,0:T(8,128)(2,1)} %add_convert_fusion, bf16[2048,1408]{1,0:T(8,128)(2,1)} %all-gather.8.cloned.1.call-done, f32[640,1408]{1,0:T(8,128)} %fusion.45), kind=kOutput, calls=%fused_computation.14 | convolution fusion | flops 7388692480 | bytes 20381696 | tf_op jit(solution)/shard_map/dot_general | solution.py:147
  381.8 0.8 dynamic_slice.32
  382.5 0.8 dynamic_slice.33
  383.3 32.1 %reduce-scatter.2.cloned.1.call-done = bf16[640,512]{1,0:T(8,128)(2,1)} async-done(((bf16[640,2048]{1,0:T(8,128)(2,1)}), bf16[640,512]{1,0:T(8,128)(2,1)}) %reduce-scatter.2.cloned.1.call-update) | async-done | bytes 655376 | tf_op jit(solution)/shard_map/reduce_scatter | solution.py:152
  415.3 1.7 fusion.7
  417.0 6.1 %all-reduce.1 = (f32[640]{0:T(1024)S(1)}, f32[640]{0:T(1024)S(1)}) all-reduce(f32[640]{0:T(1024)S(1)} %get-tuple-element.182, f32[640]{0:T(1024)S(1)} %get-tuple-element.181), channel_id=1, replica_groups=mesh['sp'=8,'tp'=4] {'tp'}, use_global_device_ids=true, to_apply=%region_16.17 | all-reduce | flops 1280 | bytes 10240 | tf_op jit(solution)/shard_map/psum | solution.py:154
  423.1 2.5 add_convert_fusion.1
  (96 shorter events, 11.5 us)
Async XLA Ops:
  7.4 73.7 %copy-start = (bf16[256,2048]{1,0:T(8,128)(2,1)S(1)}, bf16[256,2048]{1,0:T(8,128)(2,1)}, u32[]{:S(2)}) copy-start(bf16[256,2048]{1,0:T(8,128)(2,1)} %param.24) | copy-start | bytes 3145732
  7.4 5.0 %copy-start.6 = (f32[2,640]{1,0:T(2,128)S(1)}, f32[2,640]{1,0:T(2,128)}, u32[]{:S(2)}) copy-start(f32[2,640]{1,0:T(2,128)} %param.22) | copy-start | bytes 15364
  7.4 7.0 %copy-start.3 = (bf16[640,256]{1,0:T(8,128)(2,1)S(1)}, bf16[640,256]{1,0:T(8,128)(2,1)}, u32[]{:S(2)}) copy-start(bf16[640,256]{1,0:T(8,128)(2,1)} %param.20) | copy-start | bytes 983044
  7.4 138.9 %all-reduce.4.cloned.1.call-start = ((), (), s32[]{:S(2)}) async-start(), calls=%async_computation.1 | async-start | bytes 5242880 | tf_op jit(solution)/shard_map/psum | solution.py:134
  12.1 34.3 %copy-start.8 = (u32[32]{0:T(128)S(1)}, u32[32]{0:T(128)}, u32[]{:S(2)}) copy-start(u32[32]{0:T(128)} %constant.93) | copy-start | bytes 388
  77.9 3.1 copy-start.7
  83.6 96.6 %all-gather.6.cloned.1.call-start = ((), (), s32[]{:S(2)}) async-start(), calls=%async_computation.2 | async-start | bytes 6488064 | tf_op jit(solution)/shard_map/all_gather | solution.py:144
  84.1 189.0 %all-gather.10.cloned.1.call-start = ((), (), s32[]{:S(2)}) async-start(), calls=%async_computation.4 | async-start | bytes 6488064 | tf_op jit(solution)/shard_map/all_gather | solution.py:149
  84.7 280.8 %all-gather.8.cloned.1.call-start = ((), (), s32[]{:S(2)}) async-start(), calls=%async_computation.3 | async-start | bytes 6488064 | tf_op jit(solution)/shard_map/all_gather | solution.py:145
  85.3 330.0 %reduce-scatter.2.cloned.1.call-start = ((), (), s32[]{:S(2)}) async-start(), calls=%async_computation.5 | async-start | bytes 3276800 | tf_op jit(solution)/shard_map/reduce_scatter | solution.py:152
  146.3 3.7 copy-start.1
  146.3 4.2 copy-start.2
  150.0 1.8 copy-start.4
  150.0 1.8 copy-start.5
Sparse Core Ops, SparseCore 0:
  83.7 62.5 all-reduce.3
  381.9 33.4 reduce-scatter.1
Sparse Core Ops, SparseCore 1:
  86.2 93.9 all-gather.5
  182.1 91.0 all-gather.9
  275.2 90.3 all-gather.7
where the time goes:
time: 435 us; the launch traced here: 433 us
  waiting for transfers between devices  296 us (68%)
  blocking collectives  53.6 us (12%)
  matrix products  34.4 us (8%)
  other arithmetic  20.3 us (5%)
  between operations  16 us (4%)
  local copies, waits for them, and re-layouts  12.4 us (3%)
    all_gather x1, waiting for transfers between devices, shards(): lifted = add_rows(lax.all_gather(up_weight, 'sp', axis=0, tiled=True))  92.4 us
    all_gather x1, waiting for transfers between devices, shards(): lax.all_gather(down_weight, 'sp', axis=1, tiled=True)  83.6 us
    psum x1, waiting for transfers between devices, shards(): mix = lax.psum(partial_value.astype(jnp.bfloat16), 'tp')  60.8 us
    reduce_scatter x1, waiting for transfers between devices, shards(): lax.psum_scatter(terms.astype(jnp.bfloat16), 'tp', scatter_dimension=1, t...  32.1 us
    all_gather x1, blocking collectives, prefix(): lax.all_gather(part.astype(kind), axis)  26.9 us
    all_gather x1, waiting for transfers between devices, shards(): gate_acts = add_rows(lax.all_gather(gate_weight, 'sp', axis=0, tiled=True))  25.4 us
    unnamed x1, blocking collectives  20.6 us
    dot_general x1, matrix products, shards(): jnp.dot(latent_width, lax.all_gather(down_weight, 'sp', axis=1, tiled=Tru...  16.2 us
  transfers between devices with their start and end apart: 5, of which 5 were waited for; matrix products, arithmetic and copies ran while one was open for 4% of the time, Pallas kernels for 0%

commit v1 on v0

--- a/solution.py
+++ b/solution.py
@@ -1,7 +1,13 @@
+import functools
+
 import jax
 import jax.numpy as jnp
 from jax import lax
+from jax.experimental import pallas as pl
+from jax.experimental.pallas import tpu as pltpu
 from jax.sharding import PartitionSpec as P
+
+MESH = pl.DeviceIdType.MESH
 
 HD = 128
 BLOCK = 128
@@ -52,6 +58,225 @@
 
 def combine_states(earlier, later):
     return (earlier[0] * later[0], later[1] + later[0][:, None, None] * earlier[1])
+
+
+def second_norm(second_sum, width, gain, bias):
+    totals_two, squares_two = lax.psum(
+        (jnp.sum(second_sum, axis=1), jnp.sum(second_sum * second_sum, axis=1)), "tp"
+    )
+    average_two = totals_two / width
+    spread_two = squares_two / width - average_two * average_two
+    scaled_two = (second_sum - average_two[:, None]) * lax.rsqrt(spread_two + EPS)[:, None]
+    return (scaled_two * gain + bias).astype(jnp.bfloat16)
+
+
+def layer_kernel(
+    n_sp, n_tp,
+    qs_ref, ret_ref, gin_ref, state_ref, res_ref, ow_ref, gain_ref, bias_ref, g_ref, u_ref, d_ref,
+    out_ref,
+    st, ow, gw, uw, dw, mixed, settled, hidden, keep, csend, crecv, fsend, frecv,
+    st_s, st_r, ow_s, ow_r, wz_s, wy_s, w_r, mx_s, mx_r, se_s, se_r, c_s, c_r, f_s, f_r, lo,
+):
+    sp, tp = lax.axis_index("sp"), lax.axis_index("tp")
+    rows = ret_ref.shape[0]
+    outer_n = n_sp // 2
+    o, i = sp // 2, lax.rem(sp, 2)
+    x, c = tp // 2, lax.rem(tp, 2)
+    half = lax.rem(o, 2)
+    o_mate = o + 1 - 2 * half
+    sp_mate = 2 * o_mate + i
+    kr = g_ref.shape[1]
+
+    def rem_copy(src, dst, ss, rs, dev):
+        return pltpu.make_async_remote_copy(
+            src_ref=src, dst_ref=dst, send_sem=ss, recv_sem=rs, device_id=dev, device_id_type=MESH
+        )
+
+    sp_peers = [(lax.rem(sp + j, n_sp), tp) for j in range(1, n_sp)]
+    tp_peers = [(sp, lax.rem(tp + j, n_tp)) for j in range(1, n_tp)]
+    diag = (sp_mate, 2 * (1 - x) + c)
+    barrier = pltpu.get_barrier_semaphore()
+    for dev in sp_peers + tp_peers + [diag]:
+        pl.semaphore_signal(barrier, inc=1, device_id=dev, device_id_type=MESH)
+    pl.semaphore_wait(barrier, n_sp + n_tp - 1)
+
+    sends = []
+
+    def go(copy):
+        copy.start()
+        sends.append(copy)
+
+    local = [
+        pltpu.make_async_copy(state_ref, st.at[sp], lo.at[0]),
+        pltpu.make_async_copy(ow_ref, ow.at[tp], lo.at[1]),
+    ]
+    for j, dev in enumerate(sp_peers):
+        go(rem_copy(state_ref, st.at[sp], st_s.at[j], st_r.at[sp], dev))
+    for j, dev in enumerate(tp_peers):
+        go(rem_copy(ow_ref, ow.at[tp], ow_s.at[j], ow_r.at[tp], dev))
+
+    def slot(w, s):
+        if w == 2:
+            return dw.at[s]
+        return (gw, uw)[w].at[pl.ds(pl.multiple_of(s * kr, kr), kr)]
+
+    sources = (g_ref, u_ref, d_ref)
+    y_mate = (2 * o + 1 - i, tp)
+    for w in range(3):
+        for j in range(1, outer_n):
+            o_to = lax.rem(o + j, outer_n)
+            go(rem_copy(sources[w].at[lax.rem(o_to, 2)], slot(w, sp), wz_s.at[w, j], w_r.at[w, sp], (2 * o_to + i, tp)))
+        go(rem_copy(sources[w].at[half], slot(w, sp), wy_s.at[w, 0], w_r.at[w, sp], y_mate))
+        local.append(pltpu.make_async_copy(sources[w].at[half], slot(w, sp), lo.at[2 + w]))
+    for copy in local:
+        copy.start()
+
+    def arrived(w, s):
+        rem_copy(slot(w, s), slot(w, s), wy_s.at[w, 0], w_r.at[w, s], y_mate).wait_recv()
+
+    local[0].wait()
+    for j in range(1, n_sp):
+        s = lax.rem(sp + n_sp - j, n_sp)
+        rem_copy(st.at[s], st.at[s], st_s.at[0], st_r.at[s], y_mate).wait_recv()
+    heads = ret_ref.shape[1] // HD
+    for h in range(heads):
+        total = jnp.zeros((HD, HD), jnp.float32)
+        for k in range(n_sp):
+            decay = st[k, h, HD : HD + 1, :].astype(jnp.float32)
+            total = jnp.where(k < sp, total * decay + st[k, h, :HD, :].astype(jnp.float32), total)
+        entering = total.astype(jnp.bfloat16)
+        cols = slice(h * HD, (h + 1) * HD)
+        got = ret_ref[:, cols] + jnp.dot(qs_ref[:, cols], entering, preferred_element_type=jnp.float32)
+        gate = gin_ref[:, cols].astype(jnp.float32)
+        mixed[tp, :, cols] = (jax.nn.silu(gate) * head_norm(got)).astype(jnp.bfloat16)
+    for j, dev in enumerate(tp_peers):
+        go(rem_copy(mixed.at[tp], mixed.at[tp], mx_s.at[j], mx_r.at[tp], dev))
+    local[1].wait()
+    for j in range(1, n_tp):
+        t = lax.rem(tp + j, n_tp)
+        rem_copy(ow.at[t], ow.at[t], ow_s.at[0], ow_r.at[t], y_mate).wait_recv()
+        rem_copy(mixed.at[t], mixed.at[t], mx_s.at[0], mx_r.at[t], y_mate).wait_recv()
+
+    def settle(r, carry):
+        here = pl.ds(pl.multiple_of(r * BLOCK, BLOCK), BLOCK)
+        first = ALPHA * res_ref[here, :].astype(jnp.float32)
+        for t in range(n_tp):
+            first = first + jnp.dot(mixed[t, here, :], ow[t], preferred_element_type=jnp.float32)
+        center = first - jnp.mean(first, axis=1, keepdims=True)
+        spread = jnp.mean(center * center, axis=1, keepdims=True)
+        settled[0, here, :] = (center * lax.rsqrt(spread + EPS) * gain_ref[...] + bias_ref[...]).astype(jnp.bfloat16)
+        return carry
+
+    lax.fori_loop(0, rows // BLOCK, settle, 0)
+    mate = (sp_mate, tp)
+    go(rem_copy(settled.at[0], settled.at[1], se_s.at[0], se_r.at[0], mate))
+
+    for w in range(3):
+        local[2 + w].wait()
+        for j in range(1, outer_n):
+            o_from = lax.rem(o + outer_n - j, outer_n)
+            s = 2 * o_from + i
+            arrived(w, s)
+            go(rem_copy(slot(w, s), slot(w, s), wy_s.at[w, j], w_r.at[w, s], y_mate))
+        if w == 1:
+            for ww in range(2):
+                for j in range(outer_n):
+                    arrived(ww, 2 * lax.rem(o + outer_n - j, outer_n) + 1 - i)
+            chunk = rows // 2
+
+            def lift(r, carry, block):
+                here = pl.ds(pl.multiple_of(r * chunk, chunk), chunk)
+                lhs = settled[block, here, :]
+                gate = jnp.dot(lhs, gw[...], preferred_element_type=jnp.float32)
+                lifted = jnp.dot(lhs, uw[...], preferred_element_type=jnp.float32)
+                hidden[block, here, :] = (jax.nn.silu(gate) * lifted).astype(jnp.bfloat16)
+                return carry
+
+            lax.fori_loop(0, 2, functools.partial(lift, block=0), 0)
+    rem_copy(settled.at[0], settled.at[1], se_s.at[0], se_r.at[0], mate).wait_recv()
+    lax.fori_loop(0, 2, functools.partial(lift, block=1), 0)
+    for j in range(outer_n):
+        arrived(2, 2 * lax.rem(o + outer_n - j, outer_n) + 1 - i)
+
+    per_out = n_sp // n_tp
+    kc = d_ref.shape[2]
+    c_mate = (sp, 2 * x + 1 - c)
+    targets = (diag, mate, (sp, 2 * (1 - x) + c))
+
+    def finish(q):
+        rem_copy(csend.at[q], crecv.at[q], c_s.at[q], c_r.at[q], c_mate).wait_recv()
+        if q < 3:
+            fsend[q] = (keep[q].astype(jnp.float32) + crecv[q].astype(jnp.float32)).astype(jnp.bfloat16)
+            go(rem_copy(fsend.at[q], frecv.at[q], f_s.at[q], f_r.at[q], targets[q]))
+
+    for q in range(4):
+        block = 1 if q < 2 else 0
+        xb = 1 - x if q in (0, 2) else x
+
+        def project(r, carry, block=block, xb=xb, q=q):
+            here = pl.ds(pl.multiple_of(r * chunk, chunk), chunk)
+            lhs = hidden[block, here, :]
+            for k in range(per_out):
+                cols = slice(k * kc, (k + 1) * kc)
+                other = dw[(2 * xb + 1 - c) * per_out + k]
+                csend[q, here, cols] = jnp.dot(lhs, other, preferred_element_type=jnp.float32).astype(jnp.bfloat16)
+                own = dw[(2 * xb + c) * per_out + k]
+                keep[q, here, cols] = jnp.dot(lhs, own, preferred_element_type=jnp.float32).astype(jnp.bfloat16)
+            return carry
+
+        lax.fori_loop(0, 2, project, 0)
+        go(rem_copy(csend.at[q], crecv.at[q], c_s.at[q], c_r.at[q], c_mate))
+        if q > 0:
+            finish(q - 1)
+    finish(3)
+    for q in range(3):
+        rem_copy(fsend.at[q], frecv.at[q], f_s.at[q], f_r.at[q], targets[q]).wait_recv()
+    width = out_ref.shape[1]
+    mine = settled[0, :, pl.ds(pl.multiple_of(tp * width, width), width)].astype(jnp.float32)
+    total = keep[3].astype(jnp.float32) + crecv[3].astype(jnp.float32)
+    for q in range(3):
+        total = total + frecv[q].astype(jnp.float32)
+    out_ref[...] = ALPHA * mine + total
+    for copy in sends:
+        copy.wait_send()
+
+
+def fused_layer(qs, retained, gate_in, state, residual, out_weight, gain, bias, gate_w, up_w, down_w, n_sp, n_tp):
+    rows, width = residual.shape
+    kr, ff = gate_w.shape
+    hf = ff // 2
+    hw = qs.shape[1]
+    cols = width // n_tp
+    halves = lambda w: jnp.transpose(w.reshape(kr, 2, hf), (1, 0, 2))
+    down = down_w.reshape(2, hf, down_w.shape[1])
+    bf = jnp.bfloat16
+    vm, hb = pl.BlockSpec(memory_space=pltpu.VMEM), pl.BlockSpec(memory_space=pl.ANY)
+    dma = lambda *shape: pltpu.SemaphoreType.DMA(shape)
+    return pl.pallas_call(
+        functools.partial(layer_kernel, n_sp, n_tp),
+        out_shape=jax.ShapeDtypeStruct((rows, cols), jnp.float32),
+        in_specs=[vm, vm, vm, hb, vm, hb, vm, vm, hb, hb, hb],
+        out_specs=vm,
+        scratch_shapes=[
+            pltpu.VMEM((n_sp,) + state.shape, bf),
+            pltpu.VMEM((n_tp,) + out_weight.shape, bf),
+            pltpu.VMEM((n_sp * kr, hf), bf),
+            pltpu.VMEM((n_sp * kr, hf), bf),
+            pltpu.VMEM((n_sp, hf, down.shape[2]), bf),
+            pltpu.VMEM((n_tp, rows, hw), bf),
+            pltpu.VMEM((2, rows, width), bf),
+            pltpu.VMEM((2, rows, hf), bf),
+            pltpu.VMEM((4, rows, cols), bf),
+            pltpu.VMEM((4, rows, cols), bf),
+            pltpu.VMEM((4, rows, cols), bf),
+            pltpu.VMEM((3, rows, cols), bf),
+            pltpu.VMEM((3, rows, cols), bf),
+            dma(n_sp), dma(n_sp), dma(n_tp), dma(n_tp),
+            dma(3, n_sp // 2), dma(3, n_sp // 2), dma(3, n_sp),
+            dma(n_tp), dma(n_tp), dma(1), dma(1), dma(4), dma(4), dma(3), dma(3), dma(5),
+        ],
+        compiler_params=pltpu.CompilerParams(collective_id=0, has_side_effects=True, vmem_limit_bytes=63 * 1024 * 1024),
+    )(qs, retained, gate_in, state, residual, out_weight, gain[None], bias[None], halves(gate_w), halves(up_w), down)
 
 
 def shards(
@@ -112,6 +337,26 @@
     )
     before = jnp.cumsum(ending, axis=0) - ending
     device_decay = jnp.exp(jnp.sum(ending, axis=0))
+    n_sp, n_tp = lax.axis_size("sp"), lax.axis_size("tp")
+    width = residual.shape[1]
+    col_width = width // n_tp
+    col_start = lax.axis_index("tp") * col_width
+
+    def own_columns(array):
+        return lax.dynamic_slice_in_dim(array, col_start, col_width, array.ndim - 1)
+
+    if n_sp % 4 == 0 and n_tp == 4 and heads_here % 2 == 0 and gate_weight.shape[0] % 128 == 0:
+        query_wide = turned_q.astype(jnp.float32) * jnp.exp(cumul_rows)[:, :, :, None]
+        near = jnp.einsum("nihd,nhde->nihe", query_wide.astype(jnp.bfloat16), prefixes.astype(jnp.bfloat16), preferred_element_type=jnp.float32)
+        far = (query_wide * jnp.exp(before)[:, None, :, None]).astype(jnp.bfloat16)
+        tail = jnp.broadcast_to(device_decay[:, None, None], (heads_here, 16, HD))
+        state = jnp.concatenate([local_state, tail], axis=1).astype(jnp.bfloat16)
+        flat = (rows, heads_here * HD)
+        second_sum = fused_layer(
+            far.reshape(flat), (inner + near).reshape(flat), gate_input, state, residual, out_weight,
+            norm_gain, norm_bias, gate_weight, up_weight, down_weight, n_sp, n_tp,
+        )
+        return second_norm(second_sum, width, own_columns(final_gain), own_columns(final_bias))
     scanned = prefix(
         (device_decay, local_state),
         "sp",
@@ -124,13 +369,6 @@
     normed = head_norm((inner + outer).reshape(shaped)).reshape(rows, heads_here * HD)
     mixed_heads = (jax.nn.silu(gate_input.astype(jnp.float32)) * normed).astype(jnp.bfloat16)
     partial_value = jnp.dot(mixed_heads, out_weight, preferred_element_type=jnp.float32)
-    width = residual.shape[1]
-    col_width = width // lax.axis_size("tp")
-    col_start = lax.axis_index("tp") * col_width
-
-    def own_columns(array):
-        return lax.dynamic_slice_in_dim(array, col_start, col_width, array.ndim - 1)
-
     mix = lax.psum(partial_value.astype(jnp.bfloat16), "tp")
     leading_sum = ALPHA * residual.astype(jnp.float32) + mix.astype(jnp.float32)
     center = leading_sum - jnp.mean(leading_sum, axis=1, keepdims=True)
@@ -151,13 +389,7 @@
     )
     ffn_cols = lax.psum_scatter(terms.astype(jnp.bfloat16), "tp", scatter_dimension=1, tiled=True)
     second_sum = ALPHA * settled_cols.astype(jnp.float32) + ffn_cols.astype(jnp.float32)
-    totals_two, squares_two = lax.psum(
-        (jnp.sum(second_sum, axis=1), jnp.sum(second_sum * second_sum, axis=1)), "tp"
-    )
-    average_two = totals_two / width
-    spread_two = squares_two / width - average_two * average_two
-    scaled_two = (second_sum - average_two[:, None]) * lax.rsqrt(spread_two + EPS)[:, None]
-    return (scaled_two * own_columns(final_gain) + own_columns(final_bias)).astype(jnp.bfloat16)
+    return second_norm(second_sum, width, own_columns(final_gain), own_columns(final_bias))
 
 
 def solution(mesh):

time: 435 us -> 217 us (0.50)
  waiting for transfers between devices: 296 us -> 0 us
  Pallas kernels: 0 us -> 190 us
  blocking collectives: 53.6 us -> 6.27 us
  matrix products: 34.4 us -> 1.3 us
  between operations: 16 us -> 0.29 us
  other arithmetic: 20.3 us -> 7.24 us
    all_gather x3 -> x0, waiting for transfers between devices: 201 us -> none  [the longest x1 92.4 us: shards(): lifted = add_rows(lax.all_gather(up_weight, 'sp', axis=0, tiled=True))]
    pallas_call x0 -> x1, Pallas kernels: none -> 190 us  [fused_layer(): pl.pallas_call(functools.partial(layer_kernel, n_sp, n_tp), out_shape=jax...]
    psum x1 -> x0, waiting for transfers between devices: 60.8 us -> none  [shards(): mix = lax.psum(partial_value.astype(jnp.bfloat16), 'tp')]
    reduce_scatter x1 -> x0, waiting for transfers between devices: 32.1 us -> none  [shards(): lax.psum_scatter(terms.astype(jnp.bfloat16), 'tp', scatter_dimension=1, t...]
    dot_general x4 -> x1, matrix products: 31.5 us -> 0.3 us  [shards(): jnp.einsum('nihd,nhde->nihe', query_wide.astype(jnp.bfloat16), prefixes.a...]
    all_gather x1 -> x0, blocking collectives: 26.9 us -> none  [prefix(): lax.all_gather(part.astype(kind), axis)]
    unnamed x1 -> x0, blocking collectives: 20.6 us -> none
    reduce_sum x4 -> x1, other arithmetic: 6.66 us -> 1.68 us  [second_norm(): jnp.sum(second_sum, axis=1)]
  transfers between devices with their start and end apart: 5 -> 0, of which waited for: 5 -> 0; matrix products, arithmetic and copies ran while one was open for 4% -> 0% of each run, Pallas kernels for 0% -> 0%
where the time goes in v1:
time: 217 us; the launch traced here: 216 us
  Pallas kernels  190 us (88%)
  local copies, waits for them, and re-layouts  10.9 us (5%)
  other arithmetic  7.24 us (3%)
  blocking collectives  6.27 us (3%)
    pallas_call x1, Pallas kernels, fused_layer(): pl.pallas_call(functools.partial(layer_kernel, n_sp, n_tp), out_shape=jax...  190 us
    psum x1, blocking collectives, second_norm(): lax.psum((jnp.sum(second_sum, axis=1), jnp.sum(second_sum * second_sum, a...  6.27 us

profile of v1, /device:TPU:16, one launch (start us, length us, event | category | flops | bytes accessed | tf_op | source)
XLA Modules:
  0.0 216.4 jit_solution(12444805609366973805)
XLA Ops:
  0.0 0.7 reshape.149
  0.7 1.5 reduce_window_sum.24
  2.2 0.2 slice_reduce_fusion
  2.7 0.6 multiply_cosine_fusion
  3.4 1.1 copy.53
  4.6 0.2 concatenate.21
  4.9 0.2 concatenate.22
  5.1 0.2 fusion.4
  5.2 0.4 copy-done.4
  5.6 0.2 copy.54
  5.9 0.2 concatenate.24
  6.1 0.2 concatenate.25
  6.4 0.4 copy-done.3
  6.9 0.5 convolution_bitcast_fusion.1
  7.5 0.5 fusion.5
  8.0 0.8 while.14
  8.8 0.3 fusion.2
  9.1 0.5 copy.43
  9.6 0.9 copy.73
  10.5 0.2 reduce_window_sum.26
  10.9 0.9 copy.52.qs_ref
  11.9 0.6 pad_maximum_fusion.state_ref
  12.6 0.3 copy.46
  12.9 1.2 copy.47
  14.0 0.3 copy.44
  14.3 1.2 copy.45
  15.5 190.2 %shard_map.136 = f32[640,512]{1,0:T(8,128)} custom-call(bf16[640,256]{1,0:T(8,128)(2,1)} %copy.52.qs_ref, f32[640,256]{1,0:T(8,128)} %bitcast.62, bf16[640,256]{1,0:T(8,128)(2,1)} %gin_ref.1, bf16[2,144,128]{2,1,0:T(8,128)(2,1)} %pad_maximum_fusion.state_ref, bf16[640,2048]{1,0:T(8,128)(2,1)} %res_ref.1, bf16[256,2048]{1,0:T(8,128)(2,1)} %ow_ref.1, ...), custom_call_target="tpu_custom_call" | custom-call | tf_op jit(solution)/shard_map/pallas_call | solution.py:255
  205.8 1.7 fusion.24
  207.5 6.3 %all-reduce = (f32[640]{0:T(1024)S(1)}, f32[640]{0:T(1024)S(1)}) all-reduce(f32[640]{0:T(1024)S(1)} %get-tuple-element.64, f32[640]{0:T(1024)S(1)} %get-tuple-element.63), channel_id=1, replica_groups=mesh['sp'=8,'tp'=4] {'tp'}, use_global_device_ids=true, to_apply=%region_8.9 | all-reduce | flops 1280 | bytes 10240 | tf_op jit(solution)/shard_map/psum | solution.py:64
  213.8 0.8 dynamic_slice.14
  214.6 0.8 dynamic_slice.15
  215.3 1.1 add_convert_fusion
  (47 shorter events, 1.7 us)
Async XLA Ops:
  4.6 1.0 copy-start.4
  5.8 1.0 copy-start.3
  10.7 1.9 copy-start.1
  12.6 1.5 copy-start.2
  205.8 9.5 %copy-start = (f32[640,512]{1,0:T(8,128)S(1)}, f32[640,512]{1,0:T(8,128)}, u32[]{:S(2)}) copy-start(f32[640,512]{1,0:T(8,128)} %shard_map.136) | copy-start | bytes 3932164

commit v2 on v1

--- a/solution.py
+++ b/solution.py
@@ -112,8 +112,10 @@
     ]
     for j, dev in enumerate(sp_peers):
         go(rem_copy(state_ref, st.at[sp], st_s.at[j], st_r.at[sp], dev))
-    for j, dev in enumerate(tp_peers):
-        go(rem_copy(ow_ref, ow.at[tp], ow_s.at[j], ow_r.at[tp], dev))
+    c_mate, x_mate = (sp, 2 * x + 1 - c), (sp, 2 * (1 - x) + c)
+    from_c, from_x, from_d = 2 * x + 1 - c, 2 * (1 - x) + c, 2 * (1 - x) + 1 - c
+    go(rem_copy(ow_ref, ow.at[tp], ow_s.at[0], ow_r.at[tp], c_mate))
+    go(rem_copy(ow_ref, ow.at[tp], ow_s.at[1], ow_r.at[tp], x_mate))
 
     def slot(w, s):
         if w == 2:
@@ -122,10 +124,15 @@
 
     sources = (g_ref, u_ref, d_ref)
     y_mate = (2 * o + 1 - i, tp)
-    for w in range(3):
+
+    def spread(w):
         for j in range(1, outer_n):
             o_to = lax.rem(o + j, outer_n)
             go(rem_copy(sources[w].at[lax.rem(o_to, 2)], slot(w, sp), wz_s.at[w, j], w_r.at[w, sp], (2 * o_to + i, tp)))
+
+    spread(0)
+    spread(1)
+    for w in range(3):
         go(rem_copy(sources[w].at[half], slot(w, sp), wy_s.at[w, 0], w_r.at[w, sp], y_mate))
         local.append(pltpu.make_async_copy(sources[w].at[half], slot(w, sp), lo.at[2 + w]))
     for copy in local:
@@ -133,6 +140,11 @@
 
     def arrived(w, s):
         rem_copy(slot(w, s), slot(w, s), wy_s.at[w, 0], w_r.at[w, s], y_mate).wait_recv()
+
+    def hand_on(w, j):
+        s = 2 * lax.rem(o + outer_n - j, outer_n) + i
+        arrived(w, s)
+        go(rem_copy(slot(w, s), slot(w, s), wy_s.at[w, j], w_r.at[w, s], y_mate))
 
     local[0].wait()
     for j in range(1, n_sp):
@@ -149,13 +161,17 @@
         got = ret_ref[:, cols] + jnp.dot(qs_ref[:, cols], entering, preferred_element_type=jnp.float32)
         gate = gin_ref[:, cols].astype(jnp.float32)
         mixed[tp, :, cols] = (jax.nn.silu(gate) * head_norm(got)).astype(jnp.bfloat16)
-    for j, dev in enumerate(tp_peers):
-        go(rem_copy(mixed.at[tp], mixed.at[tp], mx_s.at[j], mx_r.at[tp], dev))
+    go(rem_copy(mixed.at[tp], mixed.at[tp], mx_s.at[0], mx_r.at[tp], c_mate))
+    go(rem_copy(mixed.at[tp], mixed.at[tp], mx_s.at[1], mx_r.at[tp], x_mate))
+    hand_on(0, 1)
     local[1].wait()
-    for j in range(1, n_tp):
-        t = lax.rem(tp + j, n_tp)
-        rem_copy(ow.at[t], ow.at[t], ow_s.at[0], ow_r.at[t], y_mate).wait_recv()
-        rem_copy(mixed.at[t], mixed.at[t], mx_s.at[0], mx_r.at[t], y_mate).wait_recv()
+    rem_copy(mixed.at[from_x], mixed.at[from_x], mx_s.at[2], mx_r.at[from_x], x_mate).wait_recv()
+    go(rem_copy(mixed.at[from_x], mixed.at[from_x], mx_s.at[2], mx_r.at[from_x], c_mate))
+    rem_copy(ow.at[from_x], ow.at[from_x], ow_s.at[2], ow_r.at[from_x], x_mate).wait_recv()
+    go(rem_copy(ow.at[from_x], ow.at[from_x], ow_s.at[2], ow_r.at[from_x], c_mate))
+    for t in (from_c, from_d):
+        rem_copy(ow.at[t], ow.at[t], ow_s.at[2], ow_r.at[t], c_mate).wait_recv()
+        rem_copy(mixed.at[t], mixed.at[t], mx_s.at[2], mx_r.at[t], c_mate).wait_recv()
 
     def settle(r, carry):
         here = pl.ds(pl.multiple_of(r * BLOCK, BLOCK), BLOCK)
@@ -169,38 +185,44 @@
 
     lax.fori_loop(0, rows // BLOCK, settle, 0)
     mate = (sp_mate, tp)
-    go(rem_copy(settled.at[0], settled.at[1], se_s.at[0], se_r.at[0], mate))
-
-    for w in range(3):
+    chunk = rows // 2
+    mate = (sp_mate, tp)
+
+    def part(block, k):
+        return settled.at[block, pl.ds(pl.multiple_of(k * chunk, chunk), chunk)]
+
+    go(rem_copy(part(0, c), part(1, c), se_s.at[0], se_r.at[c], mate))
+    spread(2)
+    for w in range(2):
+        for j in range(1 if w else 2, outer_n):
+            hand_on(w, j)
+    for w in range(2):
         local[2 + w].wait()
-        for j in range(1, outer_n):
-            o_from = lax.rem(o + outer_n - j, outer_n)
-            s = 2 * o_from + i
-            arrived(w, s)
-            go(rem_copy(slot(w, s), slot(w, s), wy_s.at[w, j], w_r.at[w, s], y_mate))
-        if w == 1:
-            for ww in range(2):
-                for j in range(outer_n):
-                    arrived(ww, 2 * lax.rem(o + outer_n - j, outer_n) + 1 - i)
-            chunk = rows // 2
-
-            def lift(r, carry, block):
-                here = pl.ds(pl.multiple_of(r * chunk, chunk), chunk)
-                lhs = settled[block, here, :]
-                gate = jnp.dot(lhs, gw[...], preferred_element_type=jnp.float32)
-                lifted = jnp.dot(lhs, uw[...], preferred_element_type=jnp.float32)
-                hidden[block, here, :] = (jax.nn.silu(gate) * lifted).astype(jnp.bfloat16)
-                return carry
-
-            lax.fori_loop(0, 2, functools.partial(lift, block=0), 0)
-    rem_copy(settled.at[0], settled.at[1], se_s.at[0], se_r.at[0], mate).wait_recv()
+        for j in range(outer_n):
+            arrived(w, 2 * lax.rem(o + outer_n - j, outer_n) + 1 - i)
+
+    def lift(r, carry, block):
+        here = pl.ds(pl.multiple_of(r * chunk, chunk), chunk)
+        lhs = settled[block, here, :]
+        gate = jnp.dot(lhs, gw[...], preferred_element_type=jnp.float32)
+        lifted = jnp.dot(lhs, uw[...], preferred_element_type=jnp.float32)
+        hidden[block, here, :] = (jax.nn.silu(gate) * lifted).astype(jnp.bfloat16)
+        return carry
+
+    rem_copy(part(0, c), part(1, c), se_s.at[0], se_r.at[c], mate).wait_recv()
+    go(rem_copy(part(1, c), part(1, c), se_s.at[1], se_r.at[c], c_mate))
+    lax.fori_loop(0, 2, functools.partial(lift, block=0), 0)
+    hand_on(2, 1)
+    rem_copy(part(1, 1 - c), part(1, 1 - c), se_s.at[1], se_r.at[1 - c], c_mate).wait_recv()
     lax.fori_loop(0, 2, functools.partial(lift, block=1), 0)
+    for j in range(2, outer_n):
+        hand_on(2, j)
+    local[4].wait()
     for j in range(outer_n):
         arrived(2, 2 * lax.rem(o + outer_n - j, outer_n) + 1 - i)
 
     per_out = n_sp // n_tp
     kc = d_ref.shape[2]
-    c_mate = (sp, 2 * x + 1 - c)
     targets = (diag, mate, (sp, 2 * (1 - x) + c))
 
     def finish(q):
@@ -273,7 +295,7 @@
             pltpu.VMEM((3, rows, cols), bf),
             dma(n_sp), dma(n_sp), dma(n_tp), dma(n_tp),
             dma(3, n_sp // 2), dma(3, n_sp // 2), dma(3, n_sp),
-            dma(n_tp), dma(n_tp), dma(1), dma(1), dma(4), dma(4), dma(3), dma(3), dma(5),
+            dma(n_tp), dma(n_tp), dma(2), dma(2), dma(4), dma(4), dma(3), dma(3), dma(5),
         ],
         compiler_params=pltpu.CompilerParams(collective_id=0, has_side_effects=True, vmem_limit_bytes=63 * 1024 * 1024),
     )(qs, retained, gate_in, state, residual, out_weight, gain[None], bias[None], halves(gate_w), halves(up_w), down)

time: 217 us -> 210 us (0.968)
  Pallas kernels: 190 us -> 183 us
    pallas_call x1, Pallas kernels: 190 us -> 183 us  [fused_layer(): pl.pallas_call(functools.partial(layer_kernel, n_sp, n_tp), out_shape=jax...]
where the time goes in v2:
time: 210 us
  Pallas kernels  183 us (87%)
  local copies, waits for them, and re-layouts  10.9 us (5%)
  other arithmetic  7.24 us (3%)
  blocking collectives  6.27 us (3%)
    pallas_call x1, Pallas kernels, fused_layer(): pl.pallas_call(functools.partial(layer_kernel, n_sp, n_tp), out_shape=jax...  183 us
    psum x1, blocking collectives, second_norm(): lax.psum((jnp.sum(second_sum, axis=1), jnp.sum(second_sum * second_sum, a...  6.27 us

profile of v2, /device:TPU:16, one launch (start us, length us, event | category | flops | bytes accessed | tf_op | source)
XLA Modules:
  0.0 209.5 jit_solution(4567637866314239571)
XLA Ops:
  0.0 0.7 reshape.149
  0.7 1.5 reduce_window_sum.24
  2.2 0.2 slice_reduce_fusion
  2.7 0.6 multiply_cosine_fusion
  3.4 1.1 copy.53
  4.6 0.2 concatenate.21
  4.9 0.2 concatenate.22
  5.1 0.2 fusion.4
  5.2 0.4 copy-done.4
  5.6 0.2 copy.54
  5.9 0.2 concatenate.24
  6.1 0.2 concatenate.25
  6.4 0.4 copy-done.3
  6.9 0.5 convolution_bitcast_fusion.1
  7.5 0.5 fusion.5
  8.0 0.8 while.14
  8.8 0.3 fusion.2
  9.1 0.5 copy.43
  9.6 0.9 copy.73
  10.5 0.2 reduce_window_sum.26
  10.9 0.9 copy.52.qs_ref
  11.9 0.6 pad_maximum_fusion.state_ref
  12.6 0.3 copy.46
  12.9 1.2 copy.47
  14.0 0.3 copy.44
  14.3 1.2 copy.45
  15.5 183.3 %shard_map.136 = f32[640,512]{1,0:T(8,128)} custom-call(bf16[640,256]{1,0:T(8,128)(2,1)} %copy.52.qs_ref, f32[640,256]{1,0:T(8,128)} %bitcast.62, bf16[640,256]{1,0:T(8,128)(2,1)} %gin_ref.1, bf16[2,144,128]{2,1,0:T(8,128)(2,1)} %pad_maximum_fusion.state_ref, bf16[640,2048]{1,0:T(8,128)(2,1)} %res_ref.1, bf16[256,2048]{1,0:T(8,128)(2,1)} %ow_ref.1, ...), custom_call_target="tpu_custom_call" | custom-call | tf_op jit(solution)/shard_map/pallas_call | solution.py:277
  198.9 1.7 fusion.24
  200.6 6.3 %all-reduce = (f32[640]{0:T(1024)S(1)}, f32[640]{0:T(1024)S(1)}) all-reduce(f32[640]{0:T(1024)S(1)} %get-tuple-element.64, f32[640]{0:T(1024)S(1)} %get-tuple-element.63), channel_id=1, replica_groups=mesh['sp'=8,'tp'=4] {'tp'}, use_global_device_ids=true, to_apply=%region_8.9 | all-reduce | flops 1280 | bytes 10240 | tf_op jit(solution)/shard_map/psum | solution.py:64
  206.9 0.8 dynamic_slice.14
  207.6 0.8 dynamic_slice.15
  208.4 1.1 add_convert_fusion
  (47 shorter events, 1.7 us)
Async XLA Ops:
  4.6 1.0 copy-start.4
  5.8 1.0 copy-start.3
  10.7 1.9 copy-start.1
  12.6 1.5 copy-start.2
  198.9 9.5 %copy-start = (f32[640,512]{1,0:T(8,128)S(1)}, f32[640,512]{1,0:T(8,128)}, u32[]{:S(2)}) copy-start(f32[640,512]{1,0:T(8,128)} %shard_map.136) | copy-start | bytes 3932164
